TPU v7x, 32 devices: a whole 2x2x4 slice. The times are simulated.
32 devices in a mesh: sp: 8 (over z, core), tp: 4 (over y, x).
Axes of the slice: x: 2, y: 2, z: 4, core: 2. Of those that a mesh axis runs over, the one named last changes fastest.
Arguments:
- query_a: bfloat16 [1024, 1024], P('tp', 'sp'), may hold values from -16 to 16
- key_a: bfloat16 [1024, 1024], P('tp', 'sp'), may hold values from -6 to 6
- value_a: bfloat16 [1024, 1024], P('tp', 'sp'), may hold values from -6 to 6
- cumlog_a: float32 [16, 1024], P('tp'), as said below
- query_b: bfloat16 [2048, 1024], P('tp', 'sp'), may hold values from -16 to 16
- key_b: bfloat16 [2048, 1024], P('tp', 'sp'), may hold values from -6 to 6
- value_b: bfloat16 [2048, 1024], P('tp', 'sp'), may hold values from -6 to 6
- cumlog_b: float32 [16, 1024], P('tp'), as said below
- out_weight_a: bfloat16 [1024, 2048], P('tp'), may hold values from -0.375 to 0.375
- out_weight_b: bfloat16 [2048, 2048], P('tp'), may hold values from -0.25 to 0.25
- residual: bfloat16 [1024, 2048], P(('sp', 'tp')), may hold values from -6 to 6
- norm_gain: float32 [2048], replicated, may hold values from 0.1 to 1.9
- expert_ids: int32 [1024, 2], P('sp'), may hold values from 0 to 7, as said below
- route_weight: float32 [1024, 2], P('sp'), may hold values from 0.1 to 1
- gate_w: bfloat16 [8, 2048, 1024], P('sp', None, 'tp'), may hold values from -0.125 to 0.125
- up_w: bfloat16 [8, 2048, 1024], P('sp', None, 'tp'), may hold values from -0.125 to 0.125
- down_w: bfloat16 [8, 1024, 2048], P('sp', None, 'tp'), may hold values from -0.1875 to 0.1875
Outputs:
- layer_out: bfloat16 [1024, 2048], P('sp', 'tp')
Inputs may be any that keep to these rules, and one draw needn't show every extreme that they name: `expert_ids`: each row names two different experts of one group (expert e is in group e // 2). In every aligned block of 128 rows (one index of sp) no expert is named more than 64 times, and every expert of one group, the same group for all blocks, is named exactly 64 times. `cumlog_a`: along positions the values of each head never increase. `cumlog_b`: along positions the values of each head never increase.
All inputs are finite; a program needn't handle non-finite values.
Results may differ from a plain program's by a relative error of at most 0.017.
Values may be sent and summed in bfloat16 or wider, within the bound.
A program may use at most 64 MiB of HBM per device.

v0:
```python
import jax
import jax.numpy as jnp
from jax import lax
from jax.sharding import PartitionSpec as P

HDA = 64
HDB = 128
GROUPS = 4
TOP = 2
norm_eps = 1e-05


def fold_group(state, queries, keys_piece, values_piece, cum_query, cum_key, visible, head_size):
    best, total, accum = state
    heads = best.shape[0]
    count = keys_piece.shape[1]
    key_grid = keys_piece.reshape(heads, head_size, count)
    value_grid = values_piece.reshape(heads, head_size, count)
    scores = jnp.einsum(
        "hdq,hdk->hqk", queries, key_grid, preferred_element_type=jnp.float32
    ) * head_size ** (-0.5)
    scores = scores + cum_query[:, :, None] - cum_key[:, None, :]
    scores = jnp.where(visible, scores, -jnp.inf)
    best_new = jnp.max(scores, axis=-1)
    shift = jnp.where(best_new > -jnp.inf, best_new, 0.0)
    keep_old = jnp.exp(best - shift)
    weights = jnp.exp(scores - shift[:, :, None])
    total_new = total * keep_old + jnp.sum(weights, axis=-1)
    added = jnp.einsum(
        "hqk,hdk->hdq", weights.astype(jnp.bfloat16), value_grid, preferred_element_type=jnp.float32
    )
    return (best_new, total_new, accum * keep_old[:, None, :] + added)


def empty_state(heads, head_size, length):
    return (
        jnp.full((heads, length), -jnp.inf, jnp.float32),
        jnp.zeros((heads, length), jnp.float32),
        jnp.zeros((heads, head_size, length), jnp.float32),
    )


def finish_state(state):
    accum = state[2] / state[1][:, None, :]
    return accum.astype(jnp.bfloat16).reshape(-1, accum.shape[2])


def per_device(
    query_a,
    key_a,
    value_a,
    cumlog_a,
    query_b,
    key_b,
    value_b,
    cumlog_b,
    out_weight_a,
    out_weight_b,
    residual,
    norm_gain,
    expert_ids,
    route_weight,
    gate_w,
    up_w,
    down_w,
):
    local_tokens = query_a.shape[1]
    heads_a = cumlog_a.shape[0]
    heads_b = cumlog_b.shape[0]
    my_start = lax.axis_index("sp") * local_tokens
    last_query = my_start + local_tokens - 1
    query_pos = my_start + jnp.arange(local_tokens, dtype=jnp.int32)
    cum_query_a = lax.dynamic_slice_in_dim(cumlog_a, my_start, local_tokens, 1)
    cum_query_b = lax.dynamic_slice_in_dim(cumlog_b, my_start, local_tokens, 1)
    grid_a = query_a.reshape(heads_a, HDA, local_tokens)
    grid_b = query_b.reshape(heads_b, HDB, local_tokens)
    keys_a = lax.all_gather(key_a, "sp", axis=1, tiled=True)
    vals_a = lax.all_gather(value_a, "sp", axis=1, tiled=True)
    keys_b = lax.all_gather(key_b, "sp", axis=1, tiled=True)
    vals_b = lax.all_gather(value_b, "sp", axis=1, tiled=True)
    count = keys_a.shape[1]

    def visit(state):
        key_pos = jnp.arange(count, dtype=jnp.int32)
        visible = key_pos[None, None, :] <= query_pos[None, :, None]
        new_a = fold_group(state[0], grid_a, keys_a, vals_a, cum_query_a, cumlog_a, visible, HDA)
        new_b = fold_group(state[1], grid_b, keys_b, vals_b, cum_query_b, cumlog_b, visible, HDB)
        return (new_a, new_b)

    def leave(state):
        return state

    state_a, state_b = lax.cond(
        jnp.int32(0) <= last_query,
        visit,
        leave,
        (empty_state(heads_a, HDA, local_tokens), empty_state(heads_b, HDB, local_tokens)),
    )
    attn_a = finish_state(state_a)
    attn_b = finish_state(state_b)
    term = lax.dot_general(
        attn_a, out_weight_a, (((0,), (0,)), ((), ())), preferred_element_type=jnp.float32
    )
    mixed = lax.psum_scatter(
        (
            term
            + lax.dot_general(
                attn_b, out_weight_b, (((0,), (0,)), ((), ())), preferred_element_type=jnp.float32
            )
        ).astype(jnp.bfloat16),
        "tp",
        scatter_dimension=0,
        tiled=True,
    ).astype(jnp.float32)
    summed = residual.astype(jnp.float32) + mixed
    center = summed - jnp.mean(summed, axis=-1, keepdims=True)
    variance = jnp.mean(center * center, axis=-1, keepdims=True)
    normed = (center * lax.rsqrt(variance + norm_eps) * norm_gain).astype(jnp.bfloat16)
    normed_all = lax.all_gather(normed, "tp", axis=0, tiled=True)
    experts = lax.axis_size("sp")
    group_size = experts // GROUPS
    capacity = local_tokens // group_size
    features = normed_all.shape[1]
    flat_ids = expert_ids.reshape(-1)
    marks = (flat_ids[:, None] == jnp.arange(experts, dtype=jnp.int32)[None, :]).astype(jnp.int32)
    rank = jnp.sum((jnp.cumsum(marks, axis=0) - marks) * marks, axis=1)
    slot = flat_ids * capacity + rank
    token_of = jnp.arange(local_tokens * TOP, dtype=jnp.int32) // TOP
    table = jnp.zeros((experts * capacity,), jnp.int32).at[slot].set(token_of)
    filled = jnp.zeros((experts * capacity,), jnp.bfloat16).at[slot].set(1.0)
    send = (normed_all[table] * filled[:, None]).reshape(experts, capacity, features)
    rows = lax.all_to_all(send, "sp", split_axis=0, concat_axis=0, tiled=True)
    sources, items, row_width = rows.shape
    flat_rows = rows.reshape(sources * items, row_width)
    gate = jnp.dot(flat_rows, gate_w[0], preferred_element_type=jnp.float32)
    upper = jnp.dot(flat_rows, up_w[0], preferred_element_type=jnp.float32)
    hidden = (jax.nn.silu(gate) * upper).astype(jnp.bfloat16).reshape(sources, items, -1)
    hidden_all = lax.all_gather(hidden, "tp", axis=2, tiled=True)
    result = jnp.dot(
        hidden_all.reshape(sources * items, -1), down_w[0], preferred_element_type=jnp.float32
    )
    result = result.astype(jnp.bfloat16).reshape(sources, items, -1)
    returned = lax.all_to_all(result, "sp", split_axis=0, concat_axis=0, tiled=True)
    flat_back = returned.reshape(experts * capacity, -1)
    picked = flat_back[slot].reshape(local_tokens, TOP, -1).astype(jnp.float32)
    routed = jnp.sum(picked * route_weight[:, :, None], axis=1)
    columns = routed.shape[1]
    own_cols = lax.dynamic_slice_in_dim(normed_all, lax.axis_index("tp") * columns, columns, 1)
    return (own_cols.astype(jnp.float32) + routed).astype(jnp.bfloat16)


def solution(mesh):
    placed = (
        P("tp", "sp"),
        P("tp", "sp"),
        P("tp", "sp"),
        P("tp", None),
        P("tp", "sp"),
        P("tp", "sp"),
        P("tp", "sp"),
        P("tp", None),
        P("tp", None),
        P("tp", None),
        P(("sp", "tp"), None),
        P(),
        P("sp", None),
        P("sp", None),
        P("sp", None, "tp"),
        P("sp", None, "tp"),
        P("sp", None, "tp"),
    )
    return jax.shard_map(
        per_device, mesh=mesh, in_specs=placed, out_specs=P("sp", "tp"), check_vma=False
    )
```

profile of v0, /device:TPU:0, one launch (start us, length us, event | category | flops | bytes accessed | tf_op | source)
XLA Modules:
  0.0 229.1 jit_solution(7319173430591822474)
XLA Ops:
  6.5 0.0 all-gather.4.cloned.1.call-start
  6.5 0.7 all-gather.4.cloned.1.call-update
  7.3 0.0 all-gather.6.cloned.1.call-start
  7.3 0.7 all-gather.6.cloned.1.call-update
  8.0 0.0 reduce-scatter.2.cloned.1.call-start
  8.1 0.8 copy.27
  8.8 0.1 eq.29
  9.0 0.7 eq.25
  9.7 0.7 broadcast_multiply_fusion.1
  10.4 0.1 copy.26
  10.5 0.1 mul.103
  10.6 17.6 %all_gather.18 = bf16[256,1024]{1,0:T(8,128)(2,1)S(1)} all-gather(bf16[256,128]{1,0:T(8,128)(2,1)} %param.20), channel_id=1, replica_groups=mesh['sp'=8,'tp'=4] {'sp'}, dimensions={1}, use_global_device_ids=true | all-gather | bytes 589824 | tf_op jit(solution)/shard_map/all_gather | solution.py:77
  28.2 14.7 %all_gather.19 = bf16[256,1024]{1,0:T(8,128)(2,1)S(1)} all-gather(bf16[256,128]{1,0:T(8,128)(2,1)} %param.21), channel_id=1, replica_groups=mesh['sp'=8,'tp'=4] {'sp'}, dimensions={1}, use_global_device_ids=true | all-gather | bytes 589824 | tf_op jit(solution)/shard_map/all_gather | solution.py:78
  42.9 19.9 %all-gather.6.cloned.1.call-done = bf16[512,1024]{1,0:T(8,128)(2,1)} async-done(((bf16[512,128]{1,0:T(8,128)(2,1)}), bf16[512,1024]{1,0:T(8,128)(2,1)}) %all-gather.6.cloned.1.call-update) | async-done | bytes 1048592 | tf_op jit(solution)/shard_map/all_gather | solution.py:80
  62.8 7.6 %conditional.1 = (f32[4,128]{1,0:T(4,128)S(1)}, f32[4,64,128]{2,1,0:T(8,128)S(1)}, f32[4,128]{1,0:T(4,128)S(1)}, f32[4,128,128]{2,1,0:T(8,128)S(1)}) conditional(s32[]{:T(128)} %convert_element_type.59, () %tuple.20, (s32[]{:T(128)}, s32[128]{0:T(128)S(1)}, bf16[256,128]{1,0:T(8,128)(2,1)}, bf16[256,1024]{1,0:T(8,128)(2,1)S(1)}, f32[4,1024]{1,0:T(4,128)}, ...), branch_computations={%region_0.0_spmd, %region_1.6_spmd} | conditional | flops 412324992 | bytes 26306234 | solution.py:93
  62.8 0.8 constant_dynamic-slice_fusion
  63.6 0.1 iota_compare_fusion
  63.7 1.6 fusion.27
  65.4 0.0 copy-start.6
  65.4 0.0 copy-start.10
  65.4 0.5 fusion.1
  65.9 0.6 fusion.5
  66.5 0.1 copy-done.9
  66.6 0.0 copy-done.10
  66.6 0.8 fusion.28
  67.4 0.5 fusion.3
  68.0 1.3 fusion.4
  69.3 1.1 copy.32
  70.4 1.6 fusion.29
  72.0 0.0 copy-done
  72.0 0.0 copy-start.4
  72.0 0.0 copy-start.1
  72.0 0.0 copy-start.3
  72.1 1.3 fusion.12
  73.3 0.0 reduce-scatter.2.cloned.1.call-update
  73.3 0.0 all-gather.8.cloned.1.call-start
  73.4 0.6 reduce-window.6
  74.0 0.2 slice_reduce_fusion
  74.3 0.1 fusion.21
  74.4 1.4 scatter_custom_fusion
  75.8 2.2 scatter_custom_fusion.1
  77.9 0.1 mul.105
  78.0 19.3 %reduce-scatter.2.cloned.1.call-done = bf16[32,2048]{1,0:T(8,128)(2,1)} async-done(((bf16[128,2048]{1,0:T(8,128)(2,1)}), bf16[32,2048]{1,0:T(8,128)(2,1)}) %reduce-scatter.2.cloned.1.call-update) | async-done | bytes 131088 | tf_op jit(solution)/shard_map/reduce_scatter | solution.py:104
  97.3 1.0 fusion.19
  98.4 1.1 multiply_reduce_fusion.1
  99.5 1.0 multiply_convert_fusion
  100.5 10.2 %all_gather.22 = bf16[128,2048]{1,0:T(8,128)(2,1)S(1)} all-gather(bf16[32,2048]{1,0:T(8,128)(2,1)S(1)} %multiply_convert_fusion), channel_id=1, replica_groups=mesh['sp'=8,'tp'=4] {'tp'}, dimensions={0}, use_global_device_ids=true | all-gather | bytes 655360 | tf_op jit(solution)/shard_map/all_gather | solution.py:119
  110.8 3.3 %gather_fusion = bf16[512,2048]{1,0:T(8,128)(2,1)} fusion(bf16[128,2048]{1,0:T(8,128)(2,1)S(1)} %all_gather.22, s32[1024]{0:T(1024)S(1)} %pad_clamp_fusion.1), kind=kCustom, calls=%fused_computation | custom fusion | bytes 4196352 | tf_op jit(solution)/shard_map/gather | solution.py:131
  114.1 1.8 broadcast_multiply_fusion
  115.9 0.0 copy-start.7
  115.9 53.6 %all_to_all.10 = bf16[8,64,2048]{2,1,0:T(8,128)(2,1)S(1)} all-to-all(bf16[8,64,2048]{2,1,0:T(8,128)(2,1)S(1)} %broadcast_multiply_fusion), channel_id=1, replica_groups=mesh['sp'=8,'tp'=4] {'sp'}, dimensions={0} | all-to-all | bytes 4194304 | tf_op jit(solution)/shard_map/all_to_all | solution.py:132
  169.5 0.7 fusion.16
  170.3 0.5 copy-done.8
  170.8 1.4 fusion.13
  172.2 0.0 all-gather.8.cloned.1.call-update
  172.2 24.5 %all-gather.8.cloned.1.call-done = bf16[8,64,1024]{2,1,0:T(8,128)(2,1)} async-done(((bf16[8,64,256]{2,1,0:T(8,128)(2,1)}), bf16[8,64,1024]{2,1,0:T(8,128)(2,1)}) %all-gather.8.cloned.1.call-update) | async-done | bytes 1048592 | tf_op jit(solution)/shard_map/all_gather | solution.py:138
  196.7 3.1 %convolution_convert_fusion = bf16[512,512]{1,0:T(8,128)(2,1)} fusion(bf16[512,1024]{1,0:T(8,128)(2,1)} %bitcast.66, bf16[1,1024,512]{2,1,0:T(8,128)(2,1)} %param.35), kind=kOutput, calls=%fused_computation.30 | convolution fusion | flops 537133056 | bytes 2621440 | tf_op jit(solution)/shard_map/dot_general | solution.py:139
  199.8 4.6 %all-to-all-start.1 = ((bf16[8,64,512]{2,1,0:T(8,128)(2,1)}), bf16[8,64,512]{2,1,0:T(8,128)(2,1)S(1)}, u32[]{:S(2)}, u32[]{:S(2)}) async-start(bf16[8,64,512]{2,1,0:T(8,128)(2,1)} %bitcast.57), calls=%async_computation.2 | async-start | bytes 1048576 | tf_op jit(solution)/shard_map/all_to_all | solution.py:143
  204.4 0.1 copy.29
  204.5 15.2 %all-to-all-done.1 = bf16[8,64,512]{2,1,0:T(8,128)(2,1)S(1)} async-done(((bf16[8,64,512]{2,1,0:T(8,128)(2,1)}), bf16[8,64,512]{2,1,0:T(8,128)(2,1)S(1)}, u32[]{:S(2)}, u32[]{:S(2)}) %all-to-all-start.1) | async-done | bytes 524320 | tf_op jit(solution)/shard_map/all_to_all | solution.py:143
  219.7 1.2 gather_fusion.1
  220.9 0.3 reshape.190
  221.2 0.7 multiply_reduce_fusion
  221.9 0.7 add_convert_fusion
  (32 shorter events, 0.2 us)
Async XLA Ops:
  6.5 65.5 %copy-start = (bf16[512,2048]{1,0:T(8,128)(2,1)S(1)}, bf16[512,2048]{1,0:T(8,128)(2,1)}, u32[]{:S(2)}) copy-start(bf16[512,2048]{1,0:T(8,128)(2,1)} %param.28) | copy-start | bytes 6291460
  6.5 36.4 %all-gather.4.cloned.1.call-start = ((), (), s32[]{:S(2)}) async-start(), calls=%async_computation.3 | async-start | bytes 1179648 | tf_op jit(solution)/shard_map/all_gather | solution.py:79
  7.3 55.5 %all-gather.6.cloned.1.call-start = ((), (), s32[]{:S(2)}) async-start(), calls=%async_computation.4 | async-start | bytes 1179648 | tf_op jit(solution)/shard_map/all_gather | solution.py:80
  8.0 89.3 %reduce-scatter.2.cloned.1.call-start = ((), (), s32[]{:S(2)}) async-start(), calls=%async_computation.5 | async-start | bytes 655360 | tf_op jit(solution)/shard_map/reduce_scatter | solution.py:104
  65.4 1.2 copy-start.6
  65.4 1.2 copy-start.9
  65.4 1.2 copy-start.10
  66.6 1.4 copy-start.2
  72.0 2.2 copy-start.4
  72.0 25.3 %copy-start.1 = (bf16[32,2048]{1,0:T(8,128)(2,1)S(1)}, bf16[32,2048]{1,0:T(8,128)(2,1)}, u32[]{:S(2)}) copy-start(bf16[32,2048]{1,0:T(8,128)(2,1)} %param.29) | copy-start | bytes 393220
  72.0 27.5 %copy-start.3 = (f32[2048]{0:T(1024)S(1)}, f32[2048]{0:T(1024)}, u32[]{:S(2)}) copy-start(f32[2048]{0:T(1024)} %param.30) | copy-start | bytes 24580
  73.3 123.4 %all-gather.8.cloned.1.call-start = ((), (), s32[]{:S(2)}) async-start(), calls=%async_computation.6 | async-start | bytes 1310720 | tf_op jit(solution)/shard_map/all_gather | solution.py:138
  115.9 53.6 %copy-start.7 = (bf16[1,2048,256]{2,1,0:T(8,128)(2,1)S(1)}, bf16[1,2048,256]{2,1,0:T(8,128)(2,1)}, u32[]{:S(2)}) copy-start(bf16[1,2048,256]{2,1,0:T(8,128)(2,1)} %param.33) | copy-start | bytes 3145732
  169.5 1.2 copy-start.8
  196.7 7.7 %copy-start.5 = (f32[128,2]{0,1:T(2,128)S(1)}, f32[128,2]{0,1:T(2,128)}, u32[]{:S(2)}) copy-start(f32[128,2]{0,1:T(2,128)} %param.32) | copy-start | bytes 3076
  199.8 19.9 %all-to-all-start.1 = ((bf16[8,64,512]{2,1,0:T(8,128)(2,1)}), bf16[8,64,512]{2,1,0:T(8,128)(2,1)S(1)}, u32[]{:S(2)}, u32[]{:S(2)}) async-start(bf16[8,64,512]{2,1,0:T(8,128)(2,1)} %bitcast.57), calls=%async_computation.2 | async-start | bytes 1048576 | tf_op jit(solution)/shard_map/all_to_all | solution.py:143
Sparse Core Ops, SparseCore 0:
  8.9 27.7 all-gather.3
  38.3 24.4 all-gather.5
  73.5 23.8 reduce-scatter.1
  172.3 24.3 all-gather.7
where the time goes:
time: 230 us; the launch traced here: 229 us
  blocking collectives  96.1 us (42%)
  waiting for transfers between devices  80.3 us (35%)
  between operations  13.3 us (6%)
  local copies, waits for them, and re-layouts  13.2 us (6%)
  matrix products  12.4 us (5%)
  other arithmetic  9.06 us (4%)
  starting transfers between devices  4.73 us (2%)
    all_to_all x1, blocking collectives, per_device(): rows = lax.all_to_all(send, 'sp', split_axis=0, concat_axis=0, tiled=True)  53.6 us
    all_gather x1, waiting for transfers between devices, per_device(): hidden_all = lax.all_gather(hidden, 'tp', axis=2, tiled=True)  24.5 us
    all_gather x1, waiting for transfers between devices, per_device(): vals_b = lax.all_gather(value_b, 'sp', axis=1, tiled=True)  19.9 us
    reduce_scatter x1, waiting for transfers between devices, per_device(): lax.psum_scatter((term + lax.dot_general(attn_b, out_weight_b, (((0,), (0...  19.3 us
    all_gather x1, blocking collectives, per_device(): keys_a = lax.all_gather(key_a, 'sp', axis=1, tiled=True)  17.6 us
    all_to_all x1, waiting for transfers between devices, per_device(): lax.all_to_all(result, 'sp', split_axis=0, concat_axis=0, tiled=True)  15.2 us
    all_gather x1, blocking collectives, per_device(): vals_a = lax.all_gather(value_a, 'sp', axis=1, tiled=True)  14.7 us
    all_gather x1, blocking collectives, per_device(): normed_all = lax.all_gather(normed, 'tp', axis=0, tiled=True)  10.2 us
  transfers between devices with their start and end apart: 5, of which 4 were waited for; matrix products, arithmetic and copies ran while one was open for 3% of the time, Pallas kernels for 0%

commit v1 on v0

--- a/solution.py
+++ b/solution.py
@@ -75,8 +75,11 @@
     grid_a = query_a.reshape(heads_a, HDA, local_tokens)
     grid_b = query_b.reshape(heads_b, HDB, local_tokens)
     keys_a = lax.all_gather(key_a, "sp", axis=1, tiled=True)
-    vals_a = lax.all_gather(value_a, "sp", axis=1, tiled=True)
-    keys_b = lax.all_gather(key_b, "sp", axis=1, tiled=True)
+    vals_a, keys_b = jnp.split(
+        lax.all_gather(jnp.concatenate([value_a, key_b], axis=0), "sp", axis=1, tiled=True),
+        [value_a.shape[0]],
+        axis=0,
+    )
     vals_b = lax.all_gather(value_b, "sp", axis=1, tiled=True)
     count = keys_a.shape[1]
 

time: 230 us -> 235 us (1.022)
  waiting for transfers between devices: 80.3 us -> 96.4 us
  blocking collectives: 96.1 us -> 82.2 us
    all_gather x1, waiting for transfers between devices: 0.01 us -> 29 us  [per_device(): lax.all_gather(jnp.concatenate([value_a, key_b], axis=0), 'sp', axis=1, t...]
    all_gather x1 -> x0, blocking collectives: 14.7 us -> none  [per_device(): vals_a = lax.all_gather(value_a, 'sp', axis=1, tiled=True)]
    all_gather x1, waiting for transfers between devices: 19.9 us -> 7.37 us  [per_device(): vals_b = lax.all_gather(value_b, 'sp', axis=1, tiled=True)]
    split x0 -> x2, local copies, waits for them, and re-layouts: none -> 2.42 us  [per_device(): jnp.split(lax.all_gather(jnp.concatenate([value_a, key_b], axis=0), 'sp',...]
  transfers between devices with their start and end apart: 5 -> 5, of which waited for: 4 -> 5; matrix products, arithmetic and copies ran while one was open for 3% -> 3% of each run, Pallas kernels for 0% -> 0%
where the time goes in v1:
time: 235 us
  waiting for transfers between devices  96.4 us (41%)
  blocking collectives  82.2 us (35%)
  local copies, waits for them, and re-layouts  15.1 us (6%)
  between operations  13.3 us (6%)
  matrix products  12 us (5%)
  other arithmetic  10.9 us (5%)
  starting transfers between devices  4.72 us (2%)
    all_to_all x1, blocking collectives, per_device(): rows = lax.all_to_all(send, 'sp', split_axis=0, concat_axis=0, tiled=True)  53.6 us
    all_gather x1, waiting for transfers between devices, per_device(): lax.all_gather(jnp.concatenate([value_a, key_b], axis=0), 'sp', axis=1, t...  29 us
    all_gather x1, waiting for transfers between devices, per_device(): hidden_all = lax.all_gather(hidden, 'tp', axis=2, tiled=True)  24.5 us
    reduce_scatter x1, waiting for transfers between devices, per_device(): lax.psum_scatter((term + lax.dot_general(attn_b, out_weight_b, (((0,), (0...  19.6 us
    all_gather x1, blocking collectives, per_device(): keys_a = lax.all_gather(key_a, 'sp', axis=1, tiled=True)  18.3 us
    all_to_all x1, waiting for transfers between devices, per_device(): lax.all_to_all(result, 'sp', split_axis=0, concat_axis=0, tiled=True)  15.2 us
    all_gather x1, blocking collectives, per_device(): normed_all = lax.all_gather(normed, 'tp', axis=0, tiled=True)  10.3 us
    all_gather x1, waiting for transfers between devices, per_device(): vals_b = lax.all_gather(value_b, 'sp', axis=1, tiled=True)  7.37 us
  transfers between devices with their start and end apart: 5, of which 5 were waited for; matrix products, arithmetic and copies ran while one was open for 3% of the time, Pallas kernels for 0%

profile of v1, /device:TPU:0, one launch (start us, length us, event | category | flops | bytes accessed | tf_op | source)
XLA Modules:
  0.0 234.7 jit_solution(122933380375978871)
XLA Ops:
  6.5 0.7 all-gather.6.cloned.1.call-update
  7.3 0.0 all-gather.4.cloned.1.call-start
  7.3 1.6 pad_maximum_fusion
  8.9 0.0 all-gather.4.cloned.1.call-update
  8.9 0.0 reduce-scatter.2.cloned.1.call-start
  9.0 0.8 copy.27
  9.8 0.1 eq.29
  9.9 0.6 reduce-window.6
  10.5 18.3 %all_gather.15 = bf16[256,1024]{1,0:T(8,128)(2,1)} all-gather(bf16[256,128]{1,0:T(8,128)(2,1)} %param.20), channel_id=1, replica_groups=mesh['sp'=8,'tp'=4] {'sp'}, dimensions={1}, use_global_device_ids=true | all-gather | bytes 589824 | tf_op jit(solution)/shard_map/all_gather | solution.py:77
  28.9 7.4 %all-gather.6.cloned.1.call-done = bf16[512,1024]{1,0:T(8,128)(2,1)} async-done(((bf16[512,128]{1,0:T(8,128)(2,1)}), bf16[512,1024]{1,0:T(8,128)(2,1)}) %all-gather.6.cloned.1.call-update) | async-done | bytes 1048592 | tf_op jit(solution)/shard_map/all_gather | solution.py:83
  36.2 29.0 %all-gather.4.cloned.1.call-done = bf16[768,1024]{1,0:T(8,128)(2,1)} async-done(((bf16[768,128]{1,0:T(8,128)(2,1)}), bf16[768,1024]{1,0:T(8,128)(2,1)}) %all-gather.4.cloned.1.call-update) | async-done | bytes 1572880 | tf_op jit(solution)/shard_map/all_gather | solution.py:79
  65.3 10.9 %conditional.1 = (f32[4,128]{1,0:T(4,128)S(1)}, f32[4,64,128]{2,1,0:T(8,128)}, f32[4,128]{1,0:T(4,128)S(1)}, f32[4,128,128]{2,1,0:T(8,128)S(1)}) conditional(s32[]{:T(128)} %convert_element_type.59, () %tuple.20, (s32[]{:T(128)}, s32[128]{0:T(128)S(1)}, bf16[256,128]{1,0:T(8,128)(2,1)}, bf16[256,1024]{1,0:T(8,128)(2,1)}, f32[4,1024]{1,0:T(4,128)}, ...), branch_computations={%region_0.0_spmd, %region_1.6_spmd} | conditional | flops 412324992 | bytes 25847510 | solution.py:96
  65.3 0.9 constant_dynamic-slice_fusion
  66.1 0.1 iota_compare_fusion
  66.3 0.0 copy-start.4
  66.3 1.3 split.13
  67.7 0.0 copy-done.9
  67.7 0.8 fusion.28
  68.5 0.5 fusion.3
  69.0 0.0 copy-start.8
  69.1 1.3 fusion.4
  70.4 1.1 copy.32
  71.5 1.9 fusion.27
  73.3 0.5 fusion.1
  73.9 1.1 split.12
  75.0 1.2 fusion.5
  76.2 0.9 divide_convert_fusion.1
  77.2 0.3 fusion.29
  77.5 0.0 copy-start.6
  77.5 0.0 copy-start.1
  77.5 0.0 copy-start.5
  77.5 1.3 fusion.12
  78.8 0.0 reduce-scatter.2.cloned.1.call-update
  78.8 0.0 all-gather.8.cloned.1.call-start
  78.9 0.2 slice_reduce_fusion
  79.1 0.1 eq.25
  79.3 0.1 copy.26
  79.4 0.1 mul.103
  79.6 0.1 fusion.21
  79.7 1.4 scatter_custom_fusion
  81.1 2.2 scatter_custom_fusion.1
  83.2 0.1 mul.105
  83.3 19.6 %reduce-scatter.2.cloned.1.call-done = bf16[32,2048]{1,0:T(8,128)(2,1)} async-done(((bf16[128,2048]{1,0:T(8,128)(2,1)}), bf16[32,2048]{1,0:T(8,128)(2,1)}) %reduce-scatter.2.cloned.1.call-update) | async-done | bytes 131088 | tf_op jit(solution)/shard_map/reduce_scatter | solution.py:107
  102.9 1.0 fusion.19
  104.0 1.1 multiply_reduce_fusion.1
  105.1 1.0 multiply_convert_fusion
  106.1 10.3 %all_gather.18 = bf16[128,2048]{1,0:T(8,128)(2,1)S(1)} all-gather(bf16[32,2048]{1,0:T(8,128)(2,1)S(1)} %multiply_convert_fusion), channel_id=1, replica_groups=mesh['sp'=8,'tp'=4] {'tp'}, dimensions={0}, use_global_device_ids=true | all-gather | bytes 655360 | tf_op jit(solution)/shard_map/all_gather | solution.py:122
  116.4 3.3 %gather_fusion = bf16[512,2048]{1,0:T(8,128)(2,1)} fusion(bf16[128,2048]{1,0:T(8,128)(2,1)S(1)} %all_gather.18, s32[1024]{0:T(1024)S(1)} %pad_clamp_fusion.1), kind=kCustom, calls=%fused_computation | custom fusion | bytes 4196352 | tf_op jit(solution)/shard_map/gather | solution.py:134
  119.8 1.8 broadcast_multiply_fusion
  121.6 0.0 copy-start.10
  121.6 53.6 %all_to_all.10 = bf16[8,64,2048]{2,1,0:T(8,128)(2,1)S(1)} all-to-all(bf16[8,64,2048]{2,1,0:T(8,128)(2,1)S(1)} %broadcast_multiply_fusion), channel_id=1, replica_groups=mesh['sp'=8,'tp'=4] {'sp'}, dimensions={0} | all-to-all | bytes 4194304 | tf_op jit(solution)/shard_map/all_to_all | solution.py:135
  175.1 0.7 fusion.16
  175.9 0.5 copy-done.11
  176.4 1.4 fusion.13
  177.8 0.0 all-gather.8.cloned.1.call-update
  177.8 24.5 %all-gather.8.cloned.1.call-done = bf16[8,64,1024]{2,1,0:T(8,128)(2,1)} async-done(((bf16[8,64,256]{2,1,0:T(8,128)(2,1)}), bf16[8,64,1024]{2,1,0:T(8,128)(2,1)}) %all-gather.8.cloned.1.call-update) | async-done | bytes 1048592 | tf_op jit(solution)/shard_map/all_gather | solution.py:141
  202.3 3.1 %convolution_convert_fusion = bf16[512,512]{1,0:T(8,128)(2,1)} fusion(bf16[512,1024]{1,0:T(8,128)(2,1)} %bitcast.66, bf16[1,1024,512]{2,1,0:T(8,128)(2,1)} %param.35), kind=kOutput, calls=%fused_computation.30 | convolution fusion | flops 537133056 | bytes 2621440 | tf_op jit(solution)/shard_map/dot_general | solution.py:142
  205.4 4.6 %all-to-all-start.1 = ((bf16[8,64,512]{2,1,0:T(8,128)(2,1)}), bf16[8,64,512]{2,1,0:T(8,128)(2,1)S(1)}, u32[]{:S(2)}, u32[]{:S(2)}) async-start(bf16[8,64,512]{2,1,0:T(8,128)(2,1)} %bitcast.58), calls=%async_computation.2 | async-start | bytes 1048576 | tf_op jit(solution)/shard_map/all_to_all | solution.py:146
  210.0 0.1 copy.29
  210.1 15.2 %all-to-all-done.1 = bf16[8,64,512]{2,1,0:T(8,128)(2,1)S(1)} async-done(((bf16[8,64,512]{2,1,0:T(8,128)(2,1)}), bf16[8,64,512]{2,1,0:T(8,128)(2,1)S(1)}, u32[]{:S(2)}, u32[]{:S(2)}) %all-to-all-start.1) | async-done | bytes 524320 | tf_op jit(solution)/shard_map/all_to_all | solution.py:146
  225.3 1.2 gather_fusion.1
  226.5 0.3 reshape.190
  226.8 0.7 multiply_reduce_fusion
  227.5 0.7 add_convert_fusion
  (38 shorter events, 0.2 us)
Async XLA Ops:
  6.5 71.0 %copy-start = (bf16[512,2048]{1,0:T(8,128)(2,1)S(1)}, bf16[512,2048]{1,0:T(8,128)(2,1)}, u32[]{:S(2)}) copy-start(bf16[512,2048]{1,0:T(8,128)(2,1)} %param.28) | copy-start | bytes 6291460
  6.5 29.7 %all-gather.6.cloned.1.call-start = ((), (), s32[]{:S(2)}) async-start(), calls=%async_computation.4 | async-start | bytes 1179648 | tf_op jit(solution)/shard_map/all_gather | solution.py:83
  7.3 58.0 %all-gather.4.cloned.1.call-start = ((), (), s32[]{:S(2)}) async-start(), calls=%async_computation.3 | async-start | bytes 1769472 | tf_op jit(solution)/shard_map/all_gather | solution.py:79
  8.9 94.0 %reduce-scatter.2.cloned.1.call-start = ((), (), s32[]{:S(2)}) async-start(), calls=%async_computation.5 | async-start | bytes 655360 | tf_op jit(solution)/shard_map/reduce_scatter | solution.py:107
  65.3 11.9 %copy-start.2 = (bf16[256,2048]{1,0:T(8,128)(2,1)S(1)}, bf16[256,2048]{1,0:T(8,128)(2,1)}, u32[]{:S(2)}) copy-start(bf16[256,2048]{1,0:T(8,128)(2,1)} %param.27) | copy-start | bytes 3145732
  65.3 2.4 %copy-start.9 = (f32[4,1024]{1,0:T(4,128)S(1)}, f32[4,1024]{1,0:T(4,128)}, u32[]{:S(2)}) copy-start(f32[4,1024]{1,0:T(4,128)} %get-tuple-element.156) | copy-start | bytes 49156 | tf_op jit(solution)/shard_map/cond
  65.3 2.4 %copy-start.12 = (bf16[512,128]{1,0:T(8,128)(2,1)S(1)}, bf16[512,128]{1,0:T(8,128)(2,1)}, u32[]{:S(2)}) copy-start(bf16[512,128]{1,0:T(8,128)(2,1)} %get-tuple-element.155) | copy-start | bytes 393220 | tf_op jit(solution)/shard_map/cond
  66.3 2.2 copy-start.4
  67.7 1.4 copy-start.3
  69.0 2.4 %copy-start.8 = (f32[4,1024]{1,0:T(4,128)S(1)}, f32[4,1024]{1,0:T(4,128)}, u32[]{:S(2)}) copy-start(f32[4,1024]{1,0:T(4,128)} %get-tuple-element.154) | copy-start | bytes 49156 | tf_op jit(solution)/shard_map/cond
  77.5 1.8 copy-start.6
  77.5 25.4 %copy-start.1 = (bf16[32,2048]{1,0:T(8,128)(2,1)S(1)}, bf16[32,2048]{1,0:T(8,128)(2,1)}, u32[]{:S(2)}) copy-start(bf16[32,2048]{1,0:T(8,128)(2,1)} %param.29) | copy-start | bytes 393220
  77.5 27.6 %copy-start.5 = (f32[2048]{0:T(1024)S(1)}, f32[2048]{0:T(1024)}, u32[]{:S(2)}) copy-start(f32[2048]{0:T(1024)} %param.30) | copy-start | bytes 24580
  78.8 123.5 %all-gather.8.cloned.1.call-start = ((), (), s32[]{:S(2)}) async-start(), calls=%async_computation.6 | async-start | bytes 1310720 | tf_op jit(solution)/shard_map/all_gather | solution.py:141
  121.6 53.6 %copy-start.10 = (bf16[1,2048,256]{2,1,0:T(8,128)(2,1)S(1)}, bf16[1,2048,256]{2,1,0:T(8,128)(2,1)}, u32[]{:S(2)}) copy-start(bf16[1,2048,256]{2,1,0:T(8,128)(2,1)} %param.33) | copy-start | bytes 3145732
  175.1 1.2 copy-start.11
  202.3 7.7 %copy-start.7 = (f32[128,2]{0,1:T(2,128)S(1)}, f32[128,2]{0,1:T(2,128)}, u32[]{:S(2)}) copy-start(f32[128,2]{0,1:T(2,128)} %param.32) | copy-start | bytes 3076
  205.4 19.9 %all-to-all-start.1 = ((bf16[8,64,512]{2,1,0:T(8,128)(2,1)}), bf16[8,64,512]{2,1,0:T(8,128)(2,1)S(1)}, u32[]{:S(2)}, u32[]{:S(2)}) async-start(bf16[8,64,512]{2,1,0:T(8,128)(2,1)} %bitcast.58), calls=%async_computation.2 | async-start | bytes 1048576 | tf_op jit(solution)/shard_map/all_to_all | solution.py:146
Sparse Core Ops, SparseCore 0:
  8.9 27.2 all-gather.5
  37.8 27.3 all-gather.3
  78.9 23.9 reduce-scatter.1
  177.9 24.3 all-gather.7
